TPU v7x, 32 devices: a whole 2x2x4 slice. The times are simulated.
32 devices in a mesh: sp: 16 (over z, y, core), tp: 2 (over x).
Axes of the slice: x: 2, y: 2, z: 4, core: 2. Of those that a mesh axis runs over, the one named last changes fastest.
Arguments:
- residual: bfloat16 [2048, 2048], P('sp', 'tp'), may hold values from -24 to 24
- queries: bfloat16 [2048, 2048], P('sp', 'tp'), may hold values from -16 to 16
- key_proj: bfloat16 [2048, 512], P(('sp', 'tp')), may hold values from -8 to 8
- value_proj: bfloat16 [2048, 512], P(('sp', 'tp')), may hold values from -6 to 6
- diff_lambda: float32 [8], replicated, may hold values from 0.3 to 0.8
- head_gain: float32 [256], replicated, may hold values from 0.1 to 1.9
- out_weight: bfloat16 [2048, 2048], P(None, 'tp'), may hold values from -0.125 to 0.125
- norm_gain: float32 [2048], P('tp'), may hold values from 0.1 to 1.9
- up_weight: bfloat16 [2048, 8192], P('sp', 'tp'), may hold values from -0.125 to 0.125
- down_weight: bfloat16 [8192, 2048], P('tp', 'sp'), may hold values from -0.0625 to 0.0625
Outputs:
- layer_out: bfloat16 [2048, 2048], P('sp', 'tp')
All inputs are finite; a program needn't handle non-finite values.
Results may differ from a plain program's by a relative error of at most 0.012.
Values may be sent and summed in bfloat16 or wider, within the bound.
No kernel may reach another device: no remote copies, remote signals or barrier semaphores. Data moves between devices by JAX's collectives and lax.ppermute only.
A program may use at most 128 MiB of HBM per device.

v0:
```python
import jax
import jax.numpy as jnp
from jax import lax
from jax.sharding import PartitionSpec as P

D = 2048
HEADS = 8
KV_HEADS = 2
HEAD_DIM = 128
VALUE_DIM = 256
epsilon = 1e-06


def head_norm(per_map, lambdas, gain):
    difference = per_map[:, 0] - lambdas[:, None, None] * per_map[:, 1]
    scaled = (
        difference
        * lax.rsqrt(jnp.mean(difference * difference, axis=-1, keepdims=True) + epsilon)
        * gain
    )
    return scaled.astype(jnp.bfloat16)


def on_device(
    residual,
    queries,
    key_proj,
    value_proj,
    diff_lambda,
    head_gain,
    out_weight,
    norm_gain,
    up_weight,
    down_weight,
):
    rows_here = residual.shape[0]
    per_group = HEADS // KV_HEADS
    scaling = HEAD_DIM ** (-0.5)
    all_queries = lax.all_gather(queries, "tp", axis=1, tiled=True)
    query_grid = all_queries.reshape(rows_here, KV_HEADS, per_group, 2, HEAD_DIM)
    stat_shape = (KV_HEADS, per_group, 2, rows_here)
    maxima = jnp.full(stat_shape, -1e30, jnp.float32)
    key_piece = lax.all_gather(key_proj, "sp", axis=0, tiled=True)
    value_piece = lax.all_gather(value_proj, "sp", axis=0, tiled=True)
    key_count = key_piece.shape[0]
    key_grid = key_piece.reshape(key_count, KV_HEADS, 2, HEAD_DIM)
    value_grid = value_piece.reshape(key_count, KV_HEADS, VALUE_DIM)
    scores = (
        jnp.einsum("qagcd,kacd->agcqk", query_grid, key_grid, preferred_element_type=jnp.float32)
        * scaling
    )
    highest = jnp.maximum(maxima, jnp.max(scores, axis=-1))
    weights = jnp.exp(scores - highest[..., None])
    totals = jnp.sum(weights, axis=-1)
    weighted = jnp.einsum(
        "agcqk,kae->agcqe",
        weights.astype(jnp.bfloat16),
        value_grid,
        preferred_element_type=jnp.float32,
    )
    maxima, totals, weighted = (highest, totals, weighted)
    maxima = maxima.reshape(HEADS, 2, rows_here)
    totals = totals.reshape(HEADS, 2, rows_here)
    weighted = weighted.reshape(HEADS, 2, rows_here, VALUE_DIM)
    tp_size = lax.axis_size("tp")
    local_heads = HEADS // tp_size
    got_max, got_tot, got_sum = (
        lax.all_to_all(maxima, "tp", split_axis=0, concat_axis=0, tiled=True),
        lax.all_to_all(totals, "tp", split_axis=0, concat_axis=0, tiled=True),
        lax.all_to_all(weighted, "tp", split_axis=0, concat_axis=0, tiled=True),
    )
    got_max = got_max.reshape(tp_size, local_heads, 2, rows_here)
    got_tot = got_tot.reshape(tp_size, local_heads, 2, rows_here)
    got_sum = got_sum.reshape(tp_size, local_heads, 2, rows_here, VALUE_DIM)
    highest = jnp.max(got_max, axis=0)
    factor = jnp.exp(got_max - highest)
    totals_all = jnp.sum(factor * got_tot, axis=0)
    sums_all = jnp.sum(factor[..., None] * got_sum, axis=0)
    lambdas = lax.dynamic_slice_in_dim(diff_lambda, lax.axis_index("tp") * local_heads, local_heads)
    own_heads = head_norm(sums_all / totals_all[..., None], lambdas, head_gain)
    head_outputs = lax.all_gather(own_heads, "tp", axis=0, tiled=True)
    out_grid = out_weight.reshape(HEADS, VALUE_DIM, out_weight.shape[1])
    projected = jnp.einsum(
        "hqe,hed->qd", head_outputs, out_grid, preferred_element_type=jnp.float32
    )
    after_mix = residual.astype(jnp.float32) + projected
    squares = lax.psum(jnp.sum(after_mix * after_mix, axis=1), "tp")
    normed = (after_mix * lax.rsqrt(squares / D + epsilon)[:, None] * norm_gain).astype(
        jnp.bfloat16
    )
    full_rows = lax.all_gather(normed, "tp", axis=1, tiled=True)
    hidden = jnp.dot(
        full_rows,
        lax.all_gather(up_weight, "sp", axis=0, tiled=True),
        preferred_element_type=jnp.float32,
    )
    activated = jnp.square(jax.nn.relu(hidden)).astype(jnp.bfloat16)
    partial_value = jnp.dot(
        activated,
        lax.all_gather(down_weight, "sp", axis=1, tiled=True),
        preferred_element_type=jnp.float32,
    )
    mixer_sum = lax.psum_scatter(partial_value, "tp", scatter_dimension=1, tiled=True)
    return (after_mix + mixer_sum).astype(jnp.bfloat16)


def solution(mesh):
    return jax.shard_map(
        on_device,
        mesh=mesh,
        in_specs=(
            P("sp", "tp"),
            P("sp", "tp"),
            P(("sp", "tp"), None),
            P(("sp", "tp"), None),
            P(),
            P(),
            P(None, "tp"),
            P("tp"),
            P("sp", "tp"),
            P("tp", "sp"),
        ),
        out_specs=P("sp", "tp"),
        check_vma=False,
    )
```

profile of v0, /device:TPU:0, one launch (start us, length us, event | category | flops | bytes accessed | tf_op | source)
XLA Modules:
  0.0 390.0 jit_solution(11635504555220988634)
XLA Ops:
  6.5 0.7 all-gather.5.cloned.1.call-update
  7.3 0.7 all-gather.7.cloned.1.call-update
  8.1 0.7 all-gather.11.cloned.1.call-update
  8.8 0.5 all-gather.9.cloned.1.call-update
  9.3 1.1 copy.32
  10.4 9.9 %all_gather.22 = bf16[128,2048]{0,1:T(8,128)(2,1)S(1)} all-gather(bf16[128,1024]{0,1:T(8,128)(2,1)S(1)} %copy.32), channel_id=1, replica_groups=mesh['sp'=16,'tp'=2] {'tp'}, dimensions={1}, use_global_device_ids=true | all-gather | bytes 786432 | tf_op jit(solution)/shard_map/all_gather | solution.py:39
  20.4 29.7 %all-gather.5.cloned.1.call-done = bf16[1024,512]{1,0:T(8,128)(2,1)} async-done(((bf16[64,512]{1,0:T(8,128)(2,1)}), bf16[1024,512]{1,0:T(8,128)(2,1)}) %all-gather.5.cloned.1.call-update) | async-done | bytes 1048592 | tf_op jit(solution)/shard_map/all_gather | solution.py:43
  50.1 1.5 copy.31
  51.6 4.5 %bitcast_reduce_fusion = (f32[2,4,2,128]{3,1,2,0:T(4,128)S(1)}, f32[2,2,1024,128,4]{3,2,4,1,0:T(8,128)}) fusion(bf16[1024,2,2,128,1]{0,3,4,2,1:T(8,128)(2,1)S(1)} %bitcast.61, bf16[128,2,4,2,128]{0,4,3,2,1:T(8,128)(2,1)S(1)} %bitcast.62), kind=kOutput, calls=%fused_computation.1 | convolution fusion | flops 541063168 | bytes 9969664 | tf_op jit(solution)/shard_map/qagcd,kacd->agcqk/dot_general | solution.py:49
  56.1 0.6 copy.36
  56.7 3.2 all-to-all-start
  60.0 5.6 %fusion.1 = (f32[2,4,2,128]{3,1,2,0:T(4,128)S(1)}, bf16[2,4,2,128,1024]{3,4,1,2,0:T(8,128)(2,1)}) fusion(f32[2,2,1024,128,4]{3,2,4,1,0:T(8,128)} %get-tuple-element.8, f32[2,4,2,128]{3,1,2,0:T(4,128)S(1)} %broadcast_maximum_fusion), kind=kLoop, calls=%fused_computation.3 | loop fusion | flops 8386560 | bytes 12599296 | tf_op jit(solution)/shard_map/reduce_sum | solution.py:54
  65.6 0.6 copy.41
  66.2 23.0 %all-gather.7.cloned.1.call-done = bf16[1024,512]{1,0:T(8,128)(2,1)} async-done(((bf16[64,512]{1,0:T(8,128)(2,1)}), bf16[1024,512]{1,0:T(8,128)(2,1)}) %all-gather.7.cloned.1.call-update) | async-done | bytes 1048592 | tf_op jit(solution)/shard_map/all_gather | solution.py:44
  89.1 1.5 copy.37
  90.6 3.2 all-to-all-start.2
  93.9 5.2 %fusion.5 = f32[2,4,2,128,256]{4,3,2,1,0:T(8,128)} fusion(bf16[1024,2,256,1,1]{0,2,4,3,1:T(8,128)(2,1)S(1)} %bitcast.64, bf16[2,4,2,128,1024]{3,4,1,2,0:T(8,128)(2,1)} %get-tuple-element.6), kind=kOutput, calls=%fused_computation.8 | convolution fusion | flops 1073741824 | bytes 7340032 | tf_op jit(solution)/shard_map/agcqk,kae->agcqe/dot_general | solution.py:55
  99.1 3.8 all-to-all-start.1
  103.2 25.3 %all-to-all-done.1 = f32[8,2,128,256]{3,2,1,0:T(8,128)S(1)} async-done(((f32[8,2,128,256]{3,2,1,0:T(8,128)}), f32[8,2,128,256]{3,2,1,0:T(8,128)S(1)}, u32[]{:S(2)}, u32[]{:S(2)}) %all-to-all-start.1) | async-done | bytes 2097184 | tf_op jit(solution)/shard_map/all_to_all | solution.py:70
  128.4 0.3 multiply_reduce_fusion
  128.8 0.2 broadcast_divide_fusion
  129.0 0.2 multiply_reduce_fusion.2
  129.2 0.1 multiply_convert_fusion.1
  129.4 8.5 %all_gather.24 = bf16[8,128,256]{2,1,0:T(8,128)(2,1)S(1)} all-gather(bf16[4,128,256]{2,1,0:T(8,128)(2,1)S(1)} %multiply_convert_fusion.1), channel_id=1, replica_groups=mesh['sp'=16,'tp'=2] {'tp'}, dimensions={0}, use_global_device_ids=true | all-gather | bytes 786432 | tf_op jit(solution)/shard_map/all_gather | solution.py:81
  137.9 0.8 multiply_reduce_fusion.1
  138.7 4.9 %psum.7 = f32[128]{0:T(128)S(1)} all-reduce(f32[128]{0:T(128)S(1)} %get-tuple-element.9), channel_id=1, replica_groups=mesh['sp'=16,'tp'=2] {'tp'}, use_global_device_ids=true, to_apply=%region_7.0 | all-reduce | flops 128 | bytes 1024 | tf_op jit(solution)/shard_map/psum | solution.py:87
  143.8 7.0 %all_gather.25 = bf16[128,2048]{1,0:T(8,128)(2,1)S(1)} all-gather(bf16[128,1024]{1,0:T(8,128)(2,1)S(1)} %multiply_convert_fusion), channel_id=1, replica_groups=mesh['sp'=16,'tp'=2] {'tp'}, dimensions={1}, use_global_device_ids=true | all-gather | bytes 786432 | tf_op jit(solution)/shard_map/all_gather | solution.py:91
  150.8 69.3 %all-gather.11.cloned.1.call-done = bf16[4096,2048]{1,0:T(8,128)(2,1)} async-done(((bf16[4096,128]{1,0:T(8,128)(2,1)}), bf16[4096,2048]{1,0:T(8,128)(2,1)}) %all-gather.11.cloned.1.call-update) | async-done | bytes 16777232 | tf_op jit(solution)/shard_map/all_gather | solution.py:100
  220.1 126.7 %all-gather.9.cloned.1.call-done = bf16[2048,4096]{1,0:T(8,128)(2,1)} async-done(((bf16[128,4096]{1,0:T(8,128)(2,1)}), bf16[2048,4096]{1,0:T(8,128)(2,1)}) %all-gather.9.cloned.1.call-update) | async-done | bytes 16777232 | tf_op jit(solution)/shard_map/all_gather | solution.py:94
  346.9 16.1 %fusion.8 = f32[128,2048]{1,0:T(8,128)} fusion(bf16[4096,2048]{1,0:T(8,128)(2,1)} %all-gather.11.cloned.1.call-done, bf16[128,2048]{1,0:T(8,128)(2,1)S(1)} %all_gather.25, bf16[2048,4096]{1,0:T(8,128)(2,1)} %all-gather.9.cloned.1.call-done), kind=kOutput, calls=%fused_computation.13 | convolution fusion | flops 4296540160 | bytes 35127296 | tf_op jit(solution)/shard_map/dot_general | solution.py:98
  362.9 18.7 %reduce-scatter.2.cloned.1.call-done = f32[128,1024]{1,0:T(8,128)} async-done(((f32[128,2048]{1,0:T(8,128)}), f32[128,1024]{1,0:T(8,128)}) %reduce-scatter.2.cloned.1.call-update) | async-done | bytes 524304 | tf_op jit(solution)/shard_map/reduce_scatter | solution.py:103
  381.7 1.8 add_convert_fusion
  (28 shorter events, 0.5 us)
Async XLA Ops:
  6.5 43.6 %all-gather.5.cloned.1.call-start = ((), (), s32[]{:S(2)}) async-start(), calls=%async_computation.4 | async-start | bytes 1114112 | tf_op jit(solution)/shard_map/all_gather | solution.py:43
  7.3 81.9 %all-gather.7.cloned.1.call-start = ((), (), s32[]{:S(2)}) async-start(), calls=%async_computation.5 | async-start | bytes 1114112 | tf_op jit(solution)/shard_map/all_gather | solution.py:44
  8.0 212.1 %all-gather.11.cloned.1.call-start = ((), (), s32[]{:S(2)}) async-start(), calls=%async_computation.7 | async-start | bytes 17825792 | tf_op jit(solution)/shard_map/all_gather | solution.py:100
  8.7 338.1 %all-gather.9.cloned.1.call-start = ((), (), s32[]{:S(2)}) async-start(), calls=%async_computation.6 | async-start | bytes 17825792 | tf_op jit(solution)/shard_map/all_gather | solution.py:94
  56.7 33.9 %all-to-all-start = ((f32[8,2,128]{2,1,0:T(2,128)}), f32[8,2,128]{2,1,0:T(2,128)S(1)}, u32[]{:S(2)}, u32[]{:S(2)}) async-start(f32[8,2,128]{2,1,0:T(2,128)} %copy.36), calls=%async_computation | async-start | bytes 16384 | tf_op jit(solution)/shard_map/all_to_all | solution.py:68
  90.6 8.5 %all-to-all-start.2 = ((f32[8,2,128]{2,1,0:T(2,128)}), f32[8,2,128]{2,1,0:T(2,128)S(1)}, u32[]{:S(2)}, u32[]{:S(2)}) async-start(f32[8,2,128]{2,1,0:T(2,128)} %copy.41), calls=%async_computation.2 | async-start | bytes 16384 | tf_op jit(solution)/shard_map/all_to_all | solution.py:69
  93.9 9.1 %copy-start.4 = (f32[8]{0:T(128)S(1)}, f32[8]{0:T(128)}, u32[]{:S(2)}) copy-start(f32[8]{0:T(128)} %param.14) | copy-start | bytes 100
  99.1 29.3 %all-to-all-start.1 = ((f32[8,2,128,256]{3,2,1,0:T(8,128)}), f32[8,2,128,256]{3,2,1,0:T(8,128)S(1)}, u32[]{:S(2)}, u32[]{:S(2)}) async-start(f32[8,2,128,256]{3,2,1,0:T(8,128)} %bitcast.63), calls=%async_computation.1 | async-start | bytes 4194304 | tf_op jit(solution)/shard_map/all_to_all | solution.py:70
  102.9 26.3 %copy-start.3 = (f32[256]{0:T(256)S(1)}, f32[256]{0:T(256)}, u32[]{:S(2)}) copy-start(f32[256]{0:T(256)} %param.15) | copy-start | bytes 3076
  103.0 278.7 %reduce-scatter.2.cloned.1.call-start = ((), (), s32[]{:S(2)}) async-start(), calls=%async_computation.8 | async-start | bytes 1572864 | tf_op jit(solution)/shard_map/reduce_scatter | solution.py:103
  128.4 9.4 %copy-start = (bf16[2048,1024]{1,0:T(8,128)(2,1)S(1)}, bf16[2048,1024]{1,0:T(8,128)(2,1)}, u32[]{:S(2)}) copy-start(bf16[2048,1024]{1,0:T(8,128)(2,1)} %param.16) | copy-start | bytes 12582916
  128.4 9.4 %copy-start.1 = (bf16[128,1024]{1,0:T(8,128)(2,1)S(1)}, bf16[128,1024]{1,0:T(8,128)(2,1)}, u32[]{:S(2)}) copy-start(bf16[128,1024]{1,0:T(8,128)(2,1)} %param.10) | copy-start | bytes 786436
  129.0 14.7 %copy-start.2 = (f32[1024]{0:T(1024)S(1)}, f32[1024]{0:T(1024)}, u32[]{:S(2)}) copy-start(f32[1024]{0:T(1024)} %param.17) | copy-start | bytes 12292
Sparse Core Ops, SparseCore 0:
  9.5 40.5 all-gather.4
  52.3 36.8 all-gather.6
  91.3 128.7 all-gather.10
  222.2 124.6 all-gather.8
  363.1 18.5 reduce-scatter.1
where the time goes:
time: 390 us
  waiting for transfers between devices  295 us (76%)
  blocking collectives  30.4 us (8%)
  matrix products  26.6 us (7%)
  between operations  13.3 us (3%)
  starting transfers between devices  10.4 us (3%)
  other arithmetic  8.51 us (2%)
  local copies, waits for them, and re-layouts  5.4 us (1%)
    all_gather x1, waiting for transfers between devices, on_device(): lax.all_gather(up_weight, 'sp', axis=0, tiled=True)  127 us
    all_gather x1, waiting for transfers between devices, on_device(): lax.all_gather(down_weight, 'sp', axis=1, tiled=True)  69.3 us
    all_gather x1, waiting for transfers between devices, on_device(): key_piece = lax.all_gather(key_proj, 'sp', axis=0, tiled=True)  29.7 us
    all_to_all x1, waiting for transfers between devices, on_device(): lax.all_to_all(weighted, 'tp', split_axis=0, concat_axis=0, tiled=True)  25.3 us
    all_gather x1, waiting for transfers between devices, on_device(): value_piece = lax.all_gather(value_proj, 'sp', axis=0, tiled=True)  23 us
    reduce_scatter x1, waiting for transfers between devices, on_device(): lax.psum_scatter(partial_value, 'tp', scatter_dimension=1, tiled=True)  18.7 us
    dot_general x1, matrix products, on_device(): jnp.dot(activated, lax.all_gather(down_weight, 'sp', axis=1, tiled=True),...  16.1 us
    all_gather x1, blocking collectives, on_device(): all_queries = lax.all_gather(queries, 'tp', axis=1, tiled=True)  9.94 us
  transfers between devices with their start and end apart: 8, of which 6 were waited for; matrix products, arithmetic and copies ran while one was open for 6% of the time, Pallas kernels for 0%

commit v1 on v0

--- a/solution.py
+++ b/solution.py
@@ -40,7 +40,14 @@
     query_grid = all_queries.reshape(rows_here, KV_HEADS, per_group, 2, HEAD_DIM)
     stat_shape = (KV_HEADS, per_group, 2, rows_here)
     maxima = jnp.full(stat_shape, -1e30, jnp.float32)
-    key_piece = lax.all_gather(key_proj, "sp", axis=0, tiled=True)
+    size = lax.axis_size("sp")
+    right = [(i, (i + 1) % size) for i in range(size)]
+    parts = [key_proj]
+    for far in range(1, size):
+        parts = [lax.ppermute(parts[0], "sp", right), *parts]
+    whole = jnp.concatenate(parts, axis=0)
+    offset = (lax.axis_index("sp") + 1) * parts[-1].shape[0]
+    key_piece = jnp.roll(whole, offset, axis=0)
     value_piece = lax.all_gather(value_proj, "sp", axis=0, tiled=True)
     key_count = key_piece.shape[0]
     key_grid = key_piece.reshape(key_count, KV_HEADS, 2, HEAD_DIM)

time: 390 us -> 361 us (0.926)
  waiting for transfers between devices: 295 us -> 261 us
  local copies, waits for them, and re-layouts: 5.4 us -> 11.7 us
    all_gather x1, waiting for transfers between devices: 127 us -> 0.01 us  [on_device(): lax.all_gather(up_weight, 'sp', axis=0, tiled=True)]
    ppermute x0 -> x15, waiting for transfers between devices: none -> 121 us  [on_device(): parts = [lax.ppermute(parts[0], 'sp', right), *parts]]
    all_gather x1, waiting for transfers between devices: 69.3 us -> 100 us  [on_device(): lax.all_gather(down_weight, 'sp', axis=1, tiled=True)]
    all_gather x1 -> x0, waiting for transfers between devices: 29.7 us -> none  [on_device(): key_piece = lax.all_gather(key_proj, 'sp', axis=0, tiled=True)]
    all_gather x1, waiting for transfers between devices: 23 us -> 0.01 us  [on_device(): value_piece = lax.all_gather(value_proj, 'sp', axis=0, tiled=True)]
    all_to_all x1, waiting for transfers between devices: 25.3 us -> 19 us  [on_device(): lax.all_to_all(weighted, 'tp', split_axis=0, concat_axis=0, tiled=True)]
    concatenate x0 -> x1, local copies, waits for them, and re-layouts: none -> 5.78 us  [on_device(): key_piece = jnp.roll(whole, offset, axis=0)]
  transfers between devices with their start and end apart: 8 -> 22, of which waited for: 6 -> 18; matrix products, arithmetic and copies ran while one was open for 6% -> 8% of each run, Pallas kernels for 0% -> 0%
where the time goes in v1:
time: 361 us
  waiting for transfers between devices  261 us (72%)
  blocking collectives  28.6 us (8%)
  matrix products  26.7 us (7%)
  between operations  13.4 us (4%)
  local copies, waits for them, and re-layouts  11.7 us (3%)
  starting transfers between devices  11 us (3%)
  other arithmetic  8.54 us (2%)
    ppermute x15, waiting for transfers between devices, on_device(): parts = [lax.ppermute(parts[0], 'sp', right), *parts]  121 us
    all_gather x1, waiting for transfers between devices, on_device(): lax.all_gather(down_weight, 'sp', axis=1, tiled=True)  100 us
    all_to_all x1, waiting for transfers between devices, on_device(): lax.all_to_all(weighted, 'tp', split_axis=0, concat_axis=0, tiled=True)  19 us
    reduce_scatter x1, waiting for transfers between devices, on_device(): lax.psum_scatter(partial_value, 'tp', scatter_dimension=1, tiled=True)  18.7 us
    dot_general x1, matrix products, on_device(): jnp.dot(activated, lax.all_gather(down_weight, 'sp', axis=1, tiled=True),...  16.1 us
    all_gather x1, blocking collectives, on_device(): head_outputs = lax.all_gather(own_heads, 'tp', axis=0, tiled=True)  9.47 us
    all_gather x1, blocking collectives, on_device(): full_rows = lax.all_gather(normed, 'tp', axis=1, tiled=True)  7.22 us
  transfers between devices with their start and end apart: 22, of which 18 were waited for; matrix products, arithmetic and copies ran while one was open for 8% of the time, Pallas kernels for 0%

profile of v1, /device:TPU:0, one launch (start us, length us, event | category | flops | bytes accessed | tf_op | source)
XLA Modules:
  0.0 360.6 jit_solution(1215682871849931037)
XLA Ops:
  10.2 7.6 %collective-permute-done = bf16[64,512]{0,1:T(8,128)(2,1)S(1)} collective-permute-done((bf16[64,512]{0,1:T(8,128)(2,1)S(1)}, bf16[64,512]{0,1:T(8,128)(2,1)S(1)}, u32[]{:S(2)}, u32[]{:S(2)}) %collective-permute-start) | collective-permute-done | bytes 65568 | tf_op jit(solution)/shard_map/ppermute | solution.py:47
  17.9 7.2 %collective-permute-done.1 = bf16[64,512]{0,1:T(8,128)(2,1)S(1)} collective-permute-done((bf16[64,512]{0,1:T(8,128)(2,1)S(1)}, bf16[64,512]{0,1:T(8,128)(2,1)S(1)}, u32[]{:S(2)}, u32[]{:S(2)}) %collective-permute-start.1) | collective-permute-done | bytes 65568 | tf_op jit(solution)/shard_map/ppermute | solution.py:47
  25.1 7.4 %collective-permute-done.2 = bf16[64,512]{0,1:T(8,128)(2,1)S(1)} collective-permute-done((bf16[64,512]{0,1:T(8,128)(2,1)S(1)}, bf16[64,512]{0,1:T(8,128)(2,1)S(1)}, u32[]{:S(2)}, u32[]{:S(2)}) %collective-permute-start.2) | collective-permute-done | bytes 65568 | tf_op jit(solution)/shard_map/ppermute | solution.py:47
  32.5 7.2 %collective-permute-done.3 = bf16[64,512]{0,1:T(8,128)(2,1)S(1)} collective-permute-done((bf16[64,512]{0,1:T(8,128)(2,1)S(1)}, bf16[64,512]{0,1:T(8,128)(2,1)S(1)}, u32[]{:S(2)}, u32[]{:S(2)}) %collective-permute-start.3) | collective-permute-done | bytes 65568 | tf_op jit(solution)/shard_map/ppermute | solution.py:47
  39.7 8.4 %collective-permute-done.4 = bf16[64,512]{0,1:T(8,128)(2,1)S(1)} collective-permute-done((bf16[64,512]{0,1:T(8,128)(2,1)S(1)}, bf16[64,512]{0,1:T(8,128)(2,1)S(1)}, u32[]{:S(2)}, u32[]{:S(2)}) %collective-permute-start.4) | collective-permute-done | bytes 65568 | tf_op jit(solution)/shard_map/ppermute | solution.py:47
  48.1 7.1 %collective-permute-done.5 = bf16[64,512]{0,1:T(8,128)(2,1)S(1)} collective-permute-done((bf16[64,512]{0,1:T(8,128)(2,1)S(1)}, bf16[64,512]{0,1:T(8,128)(2,1)S(1)}, u32[]{:S(2)}, u32[]{:S(2)}) %collective-permute-start.5) | collective-permute-done | bytes 65568 | tf_op jit(solution)/shard_map/ppermute | solution.py:47
  55.2 7.1 %collective-permute-done.6 = bf16[64,512]{0,1:T(8,128)(2,1)S(1)} collective-permute-done((bf16[64,512]{0,1:T(8,128)(2,1)S(1)}, bf16[64,512]{0,1:T(8,128)(2,1)S(1)}, u32[]{:S(2)}, u32[]{:S(2)}) %collective-permute-start.6) | collective-permute-done | bytes 65568 | tf_op jit(solution)/shard_map/ppermute | solution.py:47
  62.3 9.9 %collective-permute-done.7 = bf16[64,512]{0,1:T(8,128)(2,1)S(1)} collective-permute-done((bf16[64,512]{0,1:T(8,128)(2,1)S(1)}, bf16[64,512]{0,1:T(8,128)(2,1)S(1)}, u32[]{:S(2)}, u32[]{:S(2)}) %collective-permute-start.7) | collective-permute-done | bytes 65568 | tf_op jit(solution)/shard_map/ppermute | solution.py:47
  72.2 10.0 %collective-permute-done.8 = bf16[64,512]{0,1:T(8,128)(2,1)S(1)} collective-permute-done((bf16[64,512]{0,1:T(8,128)(2,1)S(1)}, bf16[64,512]{0,1:T(8,128)(2,1)S(1)}, u32[]{:S(2)}, u32[]{:S(2)}) %collective-permute-start.8) | collective-permute-done | bytes 65568 | tf_op jit(solution)/shard_map/ppermute | solution.py:47
  82.2 10.0 %collective-permute-done.9 = bf16[64,512]{0,1:T(8,128)(2,1)S(1)} collective-permute-done((bf16[64,512]{0,1:T(8,128)(2,1)S(1)}, bf16[64,512]{0,1:T(8,128)(2,1)S(1)}, u32[]{:S(2)}, u32[]{:S(2)}) %collective-permute-start.9) | collective-permute-done | bytes 65568 | tf_op jit(solution)/shard_map/ppermute | solution.py:47
  92.2 10.0 %collective-permute-done.10 = bf16[64,512]{0,1:T(8,128)(2,1)S(1)} collective-permute-done((bf16[64,512]{0,1:T(8,128)(2,1)S(1)}, bf16[64,512]{0,1:T(8,128)(2,1)S(1)}, u32[]{:S(2)}, u32[]{:S(2)}) %collective-permute-start.10) | collective-permute-done | bytes 65568 | tf_op jit(solution)/shard_map/ppermute | solution.py:47
  102.3 7.1 %collective-permute-done.11 = bf16[64,512]{0,1:T(8,128)(2,1)S(1)} collective-permute-done((bf16[64,512]{0,1:T(8,128)(2,1)S(1)}, bf16[64,512]{0,1:T(8,128)(2,1)S(1)}, u32[]{:S(2)}, u32[]{:S(2)}) %collective-permute-start.11) | collective-permute-done | bytes 65568 | tf_op jit(solution)/shard_map/ppermute | solution.py:47
  109.3 9.9 %collective-permute-done.12 = bf16[64,512]{0,1:T(8,128)(2,1)S(1)} collective-permute-done((bf16[64,512]{0,1:T(8,128)(2,1)S(1)}, bf16[64,512]{0,1:T(8,128)(2,1)S(1)}, u32[]{:S(2)}, u32[]{:S(2)}) %collective-permute-start.12) | collective-permute-done | bytes 65568 | tf_op jit(solution)/shard_map/ppermute | solution.py:47
  120.5 8.9 %collective-permute-done.13 = bf16[64,512]{0,1:T(8,128)(2,1)S(1)} collective-permute-done((bf16[64,512]{0,1:T(8,128)(2,1)S(1)}, bf16[64,512]{0,1:T(8,128)(2,1)S(1)}, u32[]{:S(2)}, u32[]{:S(2)}) %collective-permute-start.13) | collective-permute-done | bytes 65568 | tf_op jit(solution)/shard_map/ppermute | solution.py:47
  129.4 7.0 %all_gather.18 = bf16[128,2048]{0,1:T(8,128)(2,1)S(1)} all-gather(bf16[128,1024]{0,1:T(8,128)(2,1)S(1)} %copy.38), channel_id=1, replica_groups=mesh['sp'=16,'tp'=2] {'tp'}, dimensions={1}, use_global_device_ids=true | all-gather | bytes 786432 | tf_op jit(solution)/shard_map/all_gather | solution.py:39
  136.4 3.1 collective-permute-done.14
  139.5 5.8 %concatenate.6 = bf16[2048,512]{0,1:T(8,128)(2,1)S(1)} concatenate(bf16[64,512]{0,1:T(8,128)(2,1)} %collective-permute-done.14, bf16[64,512]{0,1:T(8,128)(2,1)} %copy-done.8, bf16[64,512]{0,1:T(8,128)(2,1)} %copy-done.7, bf16[64,512]{0,1:T(8,128)(2,1)} %copy-done.6, bf16[64,512]{0,1:T(8,128)(2,1)} %copy-done.5, bf16[64,512]{0,1:T(8,128)(2,1)} %copy-done.4, ...), dimensions={0} | concatenate | bytes 4194304 | tf_op jit(solution)/shard_map/jit(_roll_dynamic)/concatenate | solution.py:50
  146.0 4.5 %bitcast_reduce_fusion = (f32[2,4,2,128]{3,1,2,0:T(4,128)S(1)}, f32[2,2,1024,128,4]{3,2,4,1,0:T(8,128)}) fusion(bf16[1024,2,2,128,1]{0,3,4,2,1:T(8,128)(2,1)S(1)} %bitcast.61, bf16[128,2,4,2,128]{0,4,3,2,1:T(8,128)(2,1)S(1)} %bitcast.62), kind=kOutput, calls=%fused_computation.1 | convolution fusion | flops 541063168 | bytes 9969664 | tf_op jit(solution)/shard_map/qagcd,kacd->agcqk/dot_general | solution.py:56
  151.2 3.2 all-to-all-start
  154.4 5.7 %fusion.1 = (f32[2,4,2,128]{3,1,2,0:T(4,128)S(1)}, bf16[2,4,2,128,1024]{3,4,1,2,0:T(8,128)(2,1)}) fusion(f32[2,2,1024,128,4]{3,2,4,1,0:T(8,128)} %get-tuple-element.8, f32[2,4,2,128]{3,1,2,0:T(4,128)S(1)} %broadcast_maximum_fusion), kind=kLoop, calls=%fused_computation.3 | loop fusion | flops 8386560 | bytes 12599296 | tf_op jit(solution)/shard_map/reduce_sum | solution.py:61
  160.7 1.7 copy.43
  162.4 3.2 all-to-all-start.2
  165.7 5.2 %fusion.5 = f32[2,4,2,128,256]{4,3,2,1,0:T(8,128)} fusion(bf16[1024,2,256,1,1]{0,2,4,3,1:T(8,128)(2,1)S(1)} %bitcast.64, bf16[2,4,2,128,1024]{3,4,1,2,0:T(8,128)(2,1)} %get-tuple-element.6), kind=kOutput, calls=%fused_computation.8 | convolution fusion | flops 1073741824 | bytes 7340032 | tf_op jit(solution)/shard_map/agcqk,kae->agcqe/dot_general | solution.py:62
  170.9 3.8 %all-to-all-start.1 = ((f32[8,2,128,256]{3,2,1,0:T(8,128)}), f32[8,2,128,256]{3,2,1,0:T(8,128)S(1)}, u32[]{:S(2)}, u32[]{:S(2)}) async-start(f32[8,2,128,256]{3,2,1,0:T(8,128)} %bitcast.63), calls=%async_computation.1 | async-start | bytes 4194304 | tf_op jit(solution)/shard_map/all_to_all | solution.py:77
  174.9 19.0 %all-to-all-done.1 = f32[8,2,128,256]{3,2,1,0:T(8,128)S(1)} async-done(((f32[8,2,128,256]{3,2,1,0:T(8,128)}), f32[8,2,128,256]{3,2,1,0:T(8,128)S(1)}, u32[]{:S(2)}, u32[]{:S(2)}) %all-to-all-start.1) | async-done | bytes 2097184 | tf_op jit(solution)/shard_map/all_to_all | solution.py:77
  194.9 9.5 %all_gather.20 = bf16[8,128,256]{2,1,0:T(8,128)(2,1)S(1)} all-gather(bf16[4,128,256]{2,1,0:T(8,128)(2,1)S(1)} %multiply_convert_fusion.1), channel_id=1, replica_groups=mesh['sp'=16,'tp'=2] {'tp'}, dimensions={0}, use_global_device_ids=true | all-gather | bytes 786432 | tf_op jit(solution)/shard_map/all_gather | solution.py:88
  205.2 4.9 %psum.7 = f32[128]{0:T(128)S(1)} all-reduce(f32[128]{0:T(128)S(1)} %get-tuple-element.9), channel_id=1, replica_groups=mesh['sp'=16,'tp'=2] {'tp'}, use_global_device_ids=true, to_apply=%region_7.8 | all-reduce | flops 128 | bytes 1024 | tf_op jit(solution)/shard_map/psum | solution.py:94
  210.2 7.2 %all_gather.21 = bf16[128,2048]{1,0:T(8,128)(2,1)S(1)} all-gather(bf16[128,1024]{1,0:T(8,128)(2,1)S(1)} %multiply_convert_fusion), channel_id=1, replica_groups=mesh['sp'=16,'tp'=2] {'tp'}, dimensions={1}, use_global_device_ids=true | all-gather | bytes 786432 | tf_op jit(solution)/shard_map/all_gather | solution.py:98
  217.5 100.0 %all-gather.8.cloned.1.call-done = bf16[4096,2048]{1,0:T(8,128)(2,1)} async-done(((bf16[4096,128]{1,0:T(8,128)(2,1)}), bf16[4096,2048]{1,0:T(8,128)(2,1)}) %all-gather.8.cloned.1.call-update) | async-done | bytes 16777232 | tf_op jit(solution)/shard_map/all_gather | solution.py:107
  317.4 16.1 %fusion.8 = f32[128,2048]{1,0:T(8,128)} fusion(bf16[4096,2048]{1,0:T(8,128)(2,1)} %all-gather.8.cloned.1.call-done, bf16[128,2048]{1,0:T(8,128)(2,1)S(1)} %all_gather.21, bf16[2048,4096]{1,0:T(8,128)(2,1)} %all-gather.6.cloned.1.call-done), kind=kOutput, calls=%fused_computation.13 | convolution fusion | flops 4296540160 | bytes 35127296 | tf_op jit(solution)/shard_map/dot_general | solution.py:105
  333.6 18.7 %reduce-scatter.2.cloned.1.call-done = f32[128,1024]{1,0:T(8,128)} async-done(((f32[128,2048]{1,0:T(8,128)}), f32[128,1024]{1,0:T(8,128)}) %reduce-scatter.2.cloned.1.call-update) | async-done | bytes 524304 | tf_op jit(solution)/shard_map/reduce_scatter | solution.py:110
  352.3 1.8 add_convert_fusion
  (73 shorter events, 8.9 us)
Async XLA Ops:
  6.5 154.1 %all-gather.4.cloned.1.call-start = ((), (), s32[]{:S(2)}) async-start(), calls=%async_computation.4 | async-start | bytes 1114112 | tf_op jit(solution)/shard_map/all_gather | solution.py:51
  7.3 210.2 %all-gather.6.cloned.1.call-start = ((), (), s32[]{:S(2)}) async-start(), calls=%async_computation.5 | async-start | bytes 17825792 | tf_op jit(solution)/shard_map/all_gather | solution.py:101
  8.0 309.4 %all-gather.8.cloned.1.call-start = ((), (), s32[]{:S(2)}) async-start(), calls=%async_computation.6 | async-start | bytes 17825792 | tf_op jit(solution)/shard_map/all_gather | solution.py:107
  9.7 8.2 %collective-permute-start = (bf16[64,512]{0,1:T(8,128)(2,1)S(1)}, bf16[64,512]{0,1:T(8,128)(2,1)S(1)}, u32[]{:S(2)}, u32[]{:S(2)}) collective-permute-start(bf16[64,512]{0,1:T(8,128)(2,1)S(1)} %copy.35), channel_id=1, source_target_pairs={{0,2},{2,4},{4,6},{6,8},{8,10},{10,12},{12,14},{14,16},{16,18},{18... | collective-permute-start | bytes 196616 | tf_op jit(solution)/shard_map/ppermute | solution.py:47
  17.9 7.2 %collective-permute-start.1 = (bf16[64,512]{0,1:T(8,128)(2,1)S(1)}, bf16[64,512]{0,1:T(8,128)(2,1)S(1)}, u32[]{:S(2)}, u32[]{:S(2)}) collective-permute-start(bf16[64,512]{0,1:T(8,128)(2,1)S(1)} %collective-permute-done), channel_id=1, source_target_pairs={{0,2},{2,4},{4,6},{6,8},{8,10},{10,12},{12,14},{14,16},{16,18},{18... | collective-permute-start | bytes 196616 | tf_op jit(solution)/shard_map/ppermute | solution.py:47
  25.1 7.4 %collective-permute-start.2 = (bf16[64,512]{0,1:T(8,128)(2,1)S(1)}, bf16[64,512]{0,1:T(8,128)(2,1)S(1)}, u32[]{:S(2)}, u32[]{:S(2)}) collective-permute-start(bf16[64,512]{0,1:T(8,128)(2,1)S(1)} %collective-permute-done.1), channel_id=1, source_target_pairs={{0,2},{2,4},{4,6},{6,8},{8,10},{10,12},{12,14},{14,16},{16,18},{18... | collective-permute-start | bytes 196616 | tf_op jit(solution)/shard_map/ppermute | solution.py:47
  32.5 7.2 %collective-permute-start.3 = (bf16[64,512]{0,1:T(8,128)(2,1)S(1)}, bf16[64,512]{0,1:T(8,128)(2,1)S(1)}, u32[]{:S(2)}, u32[]{:S(2)}) collective-permute-start(bf16[64,512]{0,1:T(8,128)(2,1)S(1)} %collective-permute-done.2), channel_id=1, source_target_pairs={{0,2},{2,4},{4,6},{6,8},{8,10},{10,12},{12,14},{14,16},{16,18},{18... | collective-permute-start | bytes 196616 | tf_op jit(solution)/shard_map/ppermute | solution.py:47
  39.7 8.4 %collective-permute-start.4 = (bf16[64,512]{0,1:T(8,128)(2,1)S(1)}, bf16[64,512]{0,1:T(8,128)(2,1)S(1)}, u32[]{:S(2)}, u32[]{:S(2)}) collective-permute-start(bf16[64,512]{0,1:T(8,128)(2,1)S(1)} %collective-permute-done.3), channel_id=1, source_target_pairs={{0,2},{2,4},{4,6},{6,8},{8,10},{10,12},{12,14},{14,16},{16,18},{18... | collective-permute-start | bytes 196616 | tf_op jit(solution)/shard_map/ppermute | solution.py:47
  48.1 7.1 %collective-permute-start.5 = (bf16[64,512]{0,1:T(8,128)(2,1)S(1)}, bf16[64,512]{0,1:T(8,128)(2,1)S(1)}, u32[]{:S(2)}, u32[]{:S(2)}) collective-permute-start(bf16[64,512]{0,1:T(8,128)(2,1)S(1)} %collective-permute-done.4), channel_id=1, source_target_pairs={{0,2},{2,4},{4,6},{6,8},{8,10},{10,12},{12,14},{14,16},{16,18},{18... | collective-permute-start | bytes 196616 | tf_op jit(solution)/shard_map/ppermute | solution.py:47
  55.2 7.1 %collective-permute-start.6 = (bf16[64,512]{0,1:T(8,128)(2,1)S(1)}, bf16[64,512]{0,1:T(8,128)(2,1)S(1)}, u32[]{:S(2)}, u32[]{:S(2)}) collective-permute-start(bf16[64,512]{0,1:T(8,128)(2,1)S(1)} %collective-permute-done.5), channel_id=1, source_target_pairs={{0,2},{2,4},{4,6},{6,8},{8,10},{10,12},{12,14},{14,16},{16,18},{18... | collective-permute-start | bytes 196616 | tf_op jit(solution)/shard_map/ppermute | solution.py:47
  62.3 57.0 %copy-start.1 = (bf16[64,512]{0,1:T(8,128)(2,1)}, bf16[64,512]{0,1:T(8,128)(2,1)S(1)}, u32[]{:S(2)}) copy-start(bf16[64,512]{0,1:T(8,128)(2,1)S(1)} %collective-permute-done.6) | copy-start | bytes 196612
  62.3 9.9 %collective-permute-start.7 = (bf16[64,512]{0,1:T(8,128)(2,1)S(1)}, bf16[64,512]{0,1:T(8,128)(2,1)S(1)}, u32[]{:S(2)}, u32[]{:S(2)}) collective-permute-start(bf16[64,512]{0,1:T(8,128)(2,1)S(1)} %collective-permute-done.6), channel_id=1, source_target_pairs={{0,2},{2,4},{4,6},{6,8},{8,10},{10,12},{12,14},{14,16},{16,18},{18... | collective-permute-start | bytes 196616 | tf_op jit(solution)/shard_map/ppermute | solution.py:47
  72.2 47.1 %copy-start.2 = (bf16[64,512]{0,1:T(8,128)(2,1)}, bf16[64,512]{0,1:T(8,128)(2,1)S(1)}, u32[]{:S(2)}) copy-start(bf16[64,512]{0,1:T(8,128)(2,1)S(1)} %collective-permute-done.7) | copy-start | bytes 196612
  72.2 10.0 %collective-permute-start.8 = (bf16[64,512]{0,1:T(8,128)(2,1)S(1)}, bf16[64,512]{0,1:T(8,128)(2,1)S(1)}, u32[]{:S(2)}, u32[]{:S(2)}) collective-permute-start(bf16[64,512]{0,1:T(8,128)(2,1)S(1)} %collective-permute-done.7), channel_id=1, source_target_pairs={{0,2},{2,4},{4,6},{6,8},{8,10},{10,12},{12,14},{14,16},{16,18},{18... | collective-permute-start | bytes 196616 | tf_op jit(solution)/shard_map/ppermute | solution.py:47
  82.2 37.0 %copy-start.3 = (bf16[64,512]{0,1:T(8,128)(2,1)}, bf16[64,512]{0,1:T(8,128)(2,1)S(1)}, u32[]{:S(2)}) copy-start(bf16[64,512]{0,1:T(8,128)(2,1)S(1)} %collective-permute-done.8) | copy-start | bytes 196612
  82.2 10.0 %collective-permute-start.9 = (bf16[64,512]{0,1:T(8,128)(2,1)S(1)}, bf16[64,512]{0,1:T(8,128)(2,1)S(1)}, u32[]{:S(2)}, u32[]{:S(2)}) collective-permute-start(bf16[64,512]{0,1:T(8,128)(2,1)S(1)} %collective-permute-done.8), channel_id=1, source_target_pairs={{0,2},{2,4},{4,6},{6,8},{8,10},{10,12},{12,14},{14,16},{16,18},{18... | collective-permute-start | bytes 196616 | tf_op jit(solution)/shard_map/ppermute | solution.py:47
  92.2 27.0 %copy-start.4 = (bf16[64,512]{0,1:T(8,128)(2,1)}, bf16[64,512]{0,1:T(8,128)(2,1)S(1)}, u32[]{:S(2)}) copy-start(bf16[64,512]{0,1:T(8,128)(2,1)S(1)} %collective-permute-done.9) | copy-start | bytes 196612
  92.2 10.0 %collective-permute-start.10 = (bf16[64,512]{0,1:T(8,128)(2,1)S(1)}, bf16[64,512]{0,1:T(8,128)(2,1)S(1)}, u32[]{:S(2)}, u32[]{:S(2)}) collective-permute-start(bf16[64,512]{0,1:T(8,128)(2,1)S(1)} %collective-permute-done.9), channel_id=1, source_target_pairs={{0,2},{2,4},{4,6},{6,8},{8,10},{10,12},{12,14},{14,16},{16,18},{18... | collective-permute-start | bytes 196616 | tf_op jit(solution)/shard_map/ppermute | solution.py:47
  102.2 17.0 %copy-start.5 = (bf16[64,512]{0,1:T(8,128)(2,1)}, bf16[64,512]{0,1:T(8,128)(2,1)S(1)}, u32[]{:S(2)}) copy-start(bf16[64,512]{0,1:T(8,128)(2,1)S(1)} %collective-permute-done.10) | copy-start | bytes 196612
  102.2 7.1 %collective-permute-start.11 = (bf16[64,512]{0,1:T(8,128)(2,1)S(1)}, bf16[64,512]{0,1:T(8,128)(2,1)S(1)}, u32[]{:S(2)}, u32[]{:S(2)}) collective-permute-start(bf16[64,512]{0,1:T(8,128)(2,1)S(1)} %collective-permute-done.10), channel_id=1, source_target_pairs={{0,2},{2,4},{4,6},{6,8},{8,10},{10,12},{12,14},{14,16},{16,18},{18... | collective-permute-start | bytes 196616 | tf_op jit(solution)/shard_map/ppermute | solution.py:47
  109.3 9.9 %collective-permute-start.12 = (bf16[64,512]{0,1:T(8,128)(2,1)S(1)}, bf16[64,512]{0,1:T(8,128)(2,1)S(1)}, u32[]{:S(2)}, u32[]{:S(2)}) collective-permute-start(bf16[64,512]{0,1:T(8,128)(2,1)S(1)} %collective-permute-done.11), channel_id=1, source_target_pairs={{0,2},{2,4},{4,6},{6,8},{8,10},{10,12},{12,14},{14,16},{16,18},{18... | collective-permute-start | bytes 196616 | tf_op jit(solution)/shard_map/ppermute | solution.py:47
  119.3 17.1 %copy-start.7 = (bf16[64,512]{0,1:T(8,128)(2,1)}, bf16[64,512]{0,1:T(8,128)(2,1)S(1)}, u32[]{:S(2)}) copy-start(bf16[64,512]{0,1:T(8,128)(2,1)S(1)} %collective-permute-done.12) | copy-start | bytes 196612
  119.3 10.1 %collective-permute-start.13 = (bf16[64,512]{0,1:T(8,128)(2,1)S(1)}, bf16[64,512]{0,1:T(8,128)(2,1)S(1)}, u32[]{:S(2)}, u32[]{:S(2)}) collective-permute-start(bf16[64,512]{0,1:T(8,128)(2,1)S(1)} %collective-permute-done.12), channel_id=1, source_target_pairs={{0,2},{2,4},{4,6},{6,8},{8,10},{10,12},{12,14},{14,16},{16,18},{18... | collective-permute-start | bytes 196616 | tf_op jit(solution)/shard_map/ppermute | solution.py:47
  129.4 10.1 %collective-permute-start.14 = (bf16[64,512]{0,1:T(8,128)(2,1)S(1)}, bf16[64,512]{0,1:T(8,128)(2,1)}, u32[]{:S(2)}, u32[]{:S(2)}) collective-permute-start(bf16[64,512]{0,1:T(8,128)(2,1)S(1)} %collective-permute-done.13), channel_id=1, source_target_pairs={{0,2},{2,4},{4,6},{6,8},{8,10},{10,12},{12,14},{14,16},{16,18},{18... | collective-permute-start | bytes 196616 | tf_op jit(solution)/shard_map/ppermute | solution.py:47
  151.2 11.3 %all-to-all-start = ((f32[8,2,128]{2,1,0:T(2,128)}), f32[8,2,128]{2,1,0:T(2,128)S(1)}, u32[]{:S(2)}, u32[]{:S(2)}) async-start(f32[8,2,128]{2,1,0:T(2,128)} %copy.42), calls=%async_computation | async-start | bytes 16384 | tf_op jit(solution)/shard_map/all_to_all | solution.py:75
  162.4 8.5 %all-to-all-start.2 = ((f32[8,2,128]{2,1,0:T(2,128)}), f32[8,2,128]{2,1,0:T(2,128)S(1)}, u32[]{:S(2)}, u32[]{:S(2)}) async-start(f32[8,2,128]{2,1,0:T(2,128)} %copy.47), calls=%async_computation.2 | async-start | bytes 16384 | tf_op jit(solution)/shard_map/all_to_all | solution.py:76
  170.9 23.0 %all-to-all-start.1 = ((f32[8,2,128,256]{3,2,1,0:T(8,128)}), f32[8,2,128,256]{3,2,1,0:T(8,128)S(1)}, u32[]{:S(2)}, u32[]{:S(2)}) async-start(f32[8,2,128,256]{3,2,1,0:T(8,128)} %bitcast.63), calls=%async_computation.1 | async-start | bytes 4194304 | tf_op jit(solution)/shard_map/all_to_all | solution.py:77
  174.7 20.0 %copy-start.11 = (f32[256]{0:T(256)S(1)}, f32[256]{0:T(256)}, u32[]{:S(2)}) copy-start(f32[256]{0:T(256)} %param.15) | copy-start | bytes 3076
  174.7 177.6 %reduce-scatter.2.cloned.1.call-start = ((), (), s32[]{:S(2)}) async-start(), calls=%async_computation.7 | async-start | bytes 1572864 | tf_op jit(solution)/shard_map/reduce_scatter | solution.py:110
  193.9 10.4 %copy-start = (bf16[2048,1024]{1,0:T(8,128)(2,1)S(1)}, bf16[2048,1024]{1,0:T(8,128)(2,1)}, u32[]{:S(2)}) copy-start(bf16[2048,1024]{1,0:T(8,128)(2,1)} %param.16) | copy-start | bytes 12582916
  193.9 10.4 %copy-start.9 = (bf16[128,1024]{1,0:T(8,128)(2,1)S(1)}, bf16[128,1024]{1,0:T(8,128)(2,1)}, u32[]{:S(2)}) copy-start(bf16[128,1024]{1,0:T(8,128)(2,1)} %param.10) | copy-start | bytes 786436
  194.5 15.6 %copy-start.10 = (f32[1024]{0:T(1024)S(1)}, f32[1024]{0:T(1024)}, u32[]{:S(2)}) copy-start(f32[1024]{0:T(1024)} %param.17) | copy-start | bytes 12292
  (3 other events, 26.0 us)
Sparse Core Ops, SparseCore 0:
  9.5 41.1 all-gather.3
  52.9 132.6 all-gather.5
  187.8 129.6 all-gather.7
  333.7 18.5 reduce-scatter.1
